TPU v7x, 32 devices: a whole 2x2x4 slice. The times are simulated.
32 devices in a mesh: sp: 8 (over z, x), tp: 4 (over y, core).
Axes of the slice: x: 2, y: 2, z: 4, core: 2. Of those that a mesh axis runs over, the one named last changes fastest.
Arguments:
- moe_in: bfloat16 [1536, 2048], P('sp', 'tp'), may hold values from -6 to 6
- cotangent: bfloat16 [1536, 2048], P('sp', 'tp'), may hold values from -6 to 6
- routes: int32 [1536, 2], P('sp'), may hold values from 0 to 7, all different within a row; in each aligned block of 192 rows (0 to 191, 192 to 383, ...) at most 60 rows name the same one
- route_weight: float32 [1536, 2], P('sp'), may hold values from 0.2 to 1
- w_gate: bfloat16 [8, 3584, 2048], P('sp', 'tp'), may hold values from -0.125 to 0.125
- w_up: bfloat16 [8, 3584, 2048], P('sp', 'tp'), may hold values from -0.125 to 0.125
- w_down: bfloat16 [8, 3584, 2048], P('sp', 'tp'), may hold values from -0.09375 to 0.09375
- conv_pre: bfloat16 [1536, 2048], P('sp', 'tp'), may hold values from -6 to 6
- norm_mean: float32 [1536], P('sp'), may hold values from -3 to 3
- norm_rstd: float32 [1536], P('sp'), may hold values from 0.5 to 2
- ln_gain: float32 [2048], P('tp'), may hold values from 0.1 to 1.9
- ln_shift: float32 [2048], P('tp'), may hold values from -3 to 3
- taps: float32 [31, 2048], P(None, 'tp'), may hold values from -1 to 1
- w_proj: bfloat16 [2048, 2048], P('sp', 'tp'), may hold values from -0.125 to 0.125
Outputs:
- grad_up: bfloat16 [8, 3584, 2048], P('sp', 'tp')
- grad_down: bfloat16 [8, 3584, 2048], P('sp', 'tp')
- grad_stream: bfloat16 [1536, 2048], P('sp', 'tp')
- grad_proj: float32 [2048, 2048], P('sp', 'tp')
- grad_conv: bfloat16 [1536, 2048], P('sp', 'tp')
Inputs may be any that keep to these rules, and one draw needn't show every extreme that they name: `routes`: each token names 2 different experts. Among the tokens of one index of sp no expert is named more than 60 times, a bound that some block reaches.
All inputs are finite; a program needn't handle non-finite values.
Results may differ from a plain program's by a relative error of at most 0.02.
Values may be sent and summed in bfloat16 or wider, within the bound.
A program may use at most 64 MiB of HBM per device.

v0:
```python
import jax
import jax.numpy as jnp
from jax import lax
from jax.sharding import PartitionSpec as P


def passed_along(value, axis, steps):
    count = lax.axis_size(axis)
    first, last = (max(0, -steps), min(count, count - steps))
    return lax.ppermute(value, axis, [(source, source + steps) for source in range(first, last)])


def silu_slope(pre_value, sigmoid_value):
    return sigmoid_value * (1.0 + pre_value * (1.0 - sigmoid_value))


def expert_backward(expert_rows, routed_rows, gate_weight, up_weight, down_weight):
    gate_pre = lax.dot_general(
        expert_rows, gate_weight, (((1,), (1,)), ((), ())), preferred_element_type=jnp.float32
    )
    up_pre = lax.dot_general(
        expert_rows, up_weight, (((1,), (1,)), ((), ())), preferred_element_type=jnp.float32
    )
    gate_sigmoid = jax.nn.sigmoid(gate_pre)
    gate_active = gate_pre * gate_sigmoid
    hidden = (gate_active * up_pre).astype(jnp.bfloat16)
    hidden_grad = lax.dot_general(
        routed_rows, down_weight, (((1,), (1,)), ((), ())), preferred_element_type=jnp.float32
    )
    grad_down = lax.dot_general(
        hidden, routed_rows, (((0,), (0,)), ((), ())), preferred_element_type=jnp.float32
    ).astype(jnp.bfloat16)
    gate_grad = (hidden_grad * up_pre * silu_slope(gate_pre, gate_sigmoid)).astype(jnp.bfloat16)
    up_grad = (hidden_grad * gate_active).astype(jnp.bfloat16)
    grad_up = lax.dot_general(
        up_grad, expert_rows, (((0,), (0,)), ((), ())), preferred_element_type=jnp.float32
    ).astype(jnp.bfloat16)
    partial_rows = jnp.dot(gate_grad, gate_weight, preferred_element_type=jnp.float32)
    partial_rows = partial_rows + jnp.dot(up_grad, up_weight, preferred_element_type=jnp.float32)
    return (grad_up[None], grad_down[None], partial_rows)


def on_device(
    moe_in,
    cotangent,
    routes,
    route_weight,
    w_gate,
    w_up,
    w_down,
    conv_pre,
    norm_mean,
    norm_rstd,
    ln_gain,
    ln_shift,
    taps,
    w_proj,
):
    devices = lax.axis_size("sp")
    local_tokens = routes.shape[0]
    top_count = routes.shape[1]
    channels = moe_in.shape[1]
    capacity = 5 * local_tokens // (2 * devices)
    route_ids = routes.reshape(-1)
    onehot = (route_ids[:, None] == jnp.arange(devices, dtype=jnp.int32)[None, :]).astype(jnp.int32)
    earlier = jnp.cumsum(onehot, axis=0) - onehot
    targets = route_ids * capacity + jnp.sum(earlier * onehot, axis=1)
    positions = jnp.arange(devices * capacity, dtype=jnp.int32)
    matches = targets[None, :] == positions[:, None]
    filled = jnp.any(matches, axis=1)[:, None]
    pair_index = jnp.arange(targets.shape[0], dtype=jnp.int32)
    route_of_slot = jnp.sum(jnp.where(matches, pair_index[None, :], 0), axis=1)
    zero_value = jnp.zeros((), jnp.bfloat16)
    routed = (route_weight[:, :, None] * cotangent.astype(jnp.float32)[:, None, :]).astype(
        jnp.bfloat16
    )
    routed = routed.reshape(local_tokens * top_count, cotangent.shape[1])
    send_rows = jnp.where(filled, jnp.take(moe_in, route_of_slot // top_count, axis=0), zero_value)
    send_routed = jnp.where(filled, jnp.take(routed, route_of_slot, axis=0), zero_value)
    send_rows, send_routed = (send_rows, send_routed)
    part_rows, part_routed = (
        lax.all_to_all(send_rows, "sp", split_axis=0, concat_axis=0, tiled=True),
        lax.all_to_all(send_routed, "sp", split_axis=0, concat_axis=0, tiled=True),
    )
    expert_rows, routed_rows = (
        lax.all_gather(part_rows, "tp", axis=1, tiled=True),
        lax.all_gather(part_routed, "tp", axis=1, tiled=True),
    )
    grad_up, grad_down, partial_rows = expert_backward(
        expert_rows, routed_rows, w_gate[0], w_up[0], w_down[0]
    )
    shared = lax.psum_scatter(
        partial_rows.astype(jnp.bfloat16).astype(jnp.float32).astype(jnp.bfloat16),
        "tp",
        scatter_dimension=1,
        tiled=True,
    )
    returned = lax.all_to_all(shared, "sp", split_axis=0, concat_axis=0, tiled=True)
    picked = jnp.take(returned, targets, axis=0).astype(jnp.float32)
    grad_stream = (
        cotangent.astype(jnp.float32)
        + jnp.sum(picked.reshape(local_tokens, top_count, returned.shape[1]), axis=1)
    ).astype(jnp.bfloat16)
    mix_grad = lax.all_gather(grad_stream, "tp", axis=1, tiled=True)
    normed = (conv_pre.astype(jnp.float32) - norm_mean[:, None]) * norm_rstd[:, None]
    pre_act = normed * ln_gain[None, :] + ln_shift[None, :]
    act_sigmoid = jax.nn.sigmoid(pre_act)
    activated = (pre_act * act_sigmoid).astype(jnp.bfloat16)
    columns = mix_grad
    act_grad = jnp.dot(
        columns,
        lax.all_gather(w_proj, "sp", axis=0, tiled=True),
        preferred_element_type=jnp.float32,
    )
    columns = mix_grad
    grad_proj = lax.psum_scatter(
        lax.dot_general(
            columns, activated, (((0,), (0,)), ((), ())), preferred_element_type=jnp.float32
        ).astype(jnp.bfloat16),
        "sp",
        scatter_dimension=0,
        tiled=True,
    ).astype(jnp.float32)
    normed_grad = act_grad * silu_slope(pre_act, act_sigmoid) * ln_gain[None, :]
    first_sum, second_sum = lax.psum(
        (jnp.sum(normed_grad, axis=1), jnp.sum(normed_grad * normed, axis=1)), "tp"
    )
    width = channels * lax.axis_size("tp")
    conv_grad = norm_rstd[:, None] * (
        normed_grad - first_sum[:, None] / width - normed * (second_sum[:, None] / width)
    )
    lag_count = taps.shape[0]
    rim_rows = passed_along(conv_grad[: lag_count - 1], "sp", -1)
    extended = jnp.concatenate([conv_grad, rim_rows], axis=0)
    grad_conv = jnp.zeros((local_tokens, channels), jnp.float32)
    for lag in range(lag_count):
        grad_conv = grad_conv + taps[lag][None, :] * extended[lag : lag + local_tokens]
    return (grad_up, grad_down, grad_stream, grad_proj, grad_conv.astype(jnp.bfloat16))


def solution(mesh):
    placed = (
        P("sp", "tp"),
        P("sp", "tp"),
        P("sp", None),
        P("sp", None),
        P("sp", "tp", None),
        P("sp", "tp", None),
        P("sp", "tp", None),
        P("sp", "tp"),
        P("sp"),
        P("sp"),
        P("tp"),
        P("tp"),
        P(None, "tp"),
        P("sp", "tp"),
    )
    return jax.shard_map(
        on_device,
        mesh=mesh,
        in_specs=placed,
        out_specs=(
            P("sp", "tp", None),
            P("sp", "tp", None),
            P("sp", "tp"),
            P("sp", "tp"),
            P("sp", "tp"),
        ),
        check_vma=False,
    )
```

profile of v0, /device:TPU:0, one launch (start us, length us, event | category | flops | bytes accessed | tf_op | source)
XLA Modules:
  0.0 252.3 jit_solution(15839050493758933226)
XLA Ops:
  8.1 0.8 copy.28
  9.2 0.9 reduce-window.6
  10.0 0.2 slice_reduce_fusion
  10.4 0.2 select_reduce_fusion
  10.6 0.2 fusion.15
  10.8 1.1 mul.435
  12.0 0.5 mul.436
  12.7 0.1 mul.433
  12.9 2.1 gather_fusion
  15.2 2.1 gather_fusion.1
  17.5 0.3 select_select_fusion
  17.8 21.6 %all_to_all.30 = bf16[8,60,512]{2,1,0:T(8,128)(2,1)S(1)} all-to-all(bf16[8,60,512]{2,1,0:T(8,128)(2,1)S(1)} %get-tuple-element.44), channel_id=1, replica_groups=mesh['sp'=8,'tp'=4] {'sp'}, dimensions={0} | all-to-all | bytes 983040 | tf_op jit(solution)/shard_map/all_to_all | solution.py:82
  39.4 0.9 all_to_all.23
  40.4 17.5 %all_to_all.31 = bf16[8,60,512]{2,1,0:T(8,128)(2,1)S(1)} all-to-all(bf16[8,60,512]{2,1,0:T(8,128)(2,1)S(1)} %get-tuple-element.45), channel_id=1, replica_groups=mesh['sp'=8,'tp'=4] {'sp'}, dimensions={0} | all-to-all | bytes 983040 | tf_op jit(solution)/shard_map/all_to_all | solution.py:83
  57.9 0.9 all_to_all.21
  58.8 0.2 reduce-scatter.3.cloned.1.call-start
  59.0 2.3 all-gather.6.cloned.1.call-done
  61.4 4.9 %fusion.6 = f32[480,896]{1,0:T(8,128)S(1)} fusion(bf16[480,2048]{1,0:T(8,128)(2,1)} %all-gather.6.cloned.1.call-done, bf16[1,896,2048]{2,1,0:T(8,128)(2,1)} %param.18), kind=kOutput, calls=%fused_computation.39 | convolution fusion | flops 1761607680 | bytes 7356416 | tf_op jit(solution)/shard_map/dot_general | solution.py:18
  66.2 19.1 %all-gather.4.cloned.1.call-done = bf16[480,2048]{1,0:T(8,128)(2,1)} async-done(((bf16[480,512]{1,0:T(8,128)(2,1)}), bf16[480,2048]{1,0:T(8,128)(2,1)}) %all-gather.4.cloned.1.call-update) | async-done | bytes 1966096 | tf_op jit(solution)/shard_map/all_gather | solution.py:87
  85.4 5.1 %multiply_convert_fusion.2 = (bf16[480,896]{1,0:T(8,128)(2,1)S(1)}, f32[480,896]{1,0:T(8,128)S(1)}) fusion(f32[480,896]{1,0:T(8,128)S(1)} %fusion.6, bf16[480,2048]{1,0:T(8,128)(2,1)} %all-gather.4.cloned.1.call-done, bf16[1,896,2048]{2,1,0:T(8,128)(2,1)} %param.20), kind=kOutput, calls=%fused_computation.48 | convolution fusion | flops 1764188160 | bytes 9936896 | tf_op jit(solution)/shard_map/dot_general | solution.py:27
  90.5 0.9 copy-done.17
  91.4 2.2 fusion
  93.6 2.3 fusion.2
  95.9 1.2 copy-done.16
  97.1 3.7 %add_convert_fusion = bf16[480,2048]{1,0:T(8,128)(2,1)} fusion(f32[480,2048]{1,0:T(8,128)S(1)} %fusion, bf16[1,896,2048]{2,1,0:T(8,128)(2,1)S(1)} %copy-done.10, f32[480,896]{1,0:T(8,128)S(1)} %fusion.6, f32[480,896]{1,0:T(8,128)S(1)} %get-tuple-element.47, f32[480,896]{1,0:T(8,128)S(1)} %fusion.2), kind=kOutput, calls=%fused_computation.32 | convolution fusion | flops 1767874560 | bytes 14729216 | tf_op jit(solution)/shard_map/dot_general | solution.py:38
  100.9 0.5 all-gather.8.cloned.1.call-update
  101.4 30.0 %reduce-scatter.3.cloned.1.call-done = bf16[480,512]{1,0:T(8,128)(2,1)} async-done(((bf16[480,2048]{1,0:T(8,128)(2,1)}), bf16[480,512]{1,0:T(8,128)(2,1)}) %reduce-scatter.3.cloned.1.call-update) | async-done | bytes 491536 | tf_op jit(solution)/shard_map/reduce_scatter | solution.py:92
  131.4 1.9 all_to_all.24
  133.3 5.5 %all-to-all-start.2 = ((bf16[8,60,512]{2,1,0:T(8,128)(2,1)}), bf16[8,60,512]{2,1,0:T(8,128)(2,1)S(1)}, u32[]{:S(2)}, u32[]{:S(2)}) async-start(bf16[8,60,512]{2,1,0:T(8,128)(2,1)} %all_to_all.24), calls=%async_computation.3 | async-start | bytes 1048576 | tf_op jit(solution)/shard_map/all_to_all | solution.py:98
  139.2 0.1 mul.447
  139.4 0.2 copy.32
  139.6 21.8 %all-to-all-done.2 = bf16[8,60,512]{2,1,0:T(8,128)(2,1)S(1)} async-done(((bf16[8,60,512]{2,1,0:T(8,128)(2,1)}), bf16[8,60,512]{2,1,0:T(8,128)(2,1)S(1)}, u32[]{:S(2)}, u32[]{:S(2)}) %all-to-all-start.2) | async-done | bytes 491552 | tf_op jit(solution)/shard_map/all_to_all | solution.py:98
  161.5 2.1 gather_fusion.2
  163.6 0.2 gather.23
  163.8 1.1 convert_reduce_fusion
  165.0 8.4 %all_gather.14 = bf16[192,2048]{1,0:T(8,128)(2,1)S(1)} all-gather(bf16[192,512]{1,0:T(8,128)(2,1)S(1)} %add_convert_fusion.1), channel_id=1, replica_groups=mesh['sp'=8,'tp'=4] {'tp'}, dimensions={1}, use_global_device_ids=true | all-gather | bytes 983040 | tf_op jit(solution)/shard_map/all_gather | solution.py:104
  173.4 2.3 convolution_convert_fusion
  175.7 0.8 copy-done.4
  176.6 0.7 copy-done.12
  177.3 6.0 %convert_bitcast_fusion = bf16[1,896,2048]{2,1,0:T(8,128)(2,1)} fusion(bf16[480,2048]{1,0:T(8,128)(2,1)S(1)} %copy-done.12, f32[480,896]{1,0:T(8,128)} %copy-done.16, f32[480,896]{1,0:T(8,128)} %copy-done.15), kind=kOutput, calls=%fused_computation.43 | convolution fusion | flops 1766023168 | bytes 9076736 | tf_op jit(solution)/shard_map/dot_general | solution.py:30
  183.3 2.5 fusion.121
  185.8 7.0 %all-reduce = (f32[192]{0:T(256)S(1)}, f32[192]{0:T(256)S(1)}) all-reduce(f32[192]{0:T(256)S(1)} %get-tuple-element.6, f32[192]{0:T(256)S(1)} %get-tuple-element.5), channel_id=1, replica_groups=mesh['sp'=8,'tp'=4] {'tp'}, use_global_device_ids=true, to_apply=%region_11.12 | all-reduce | flops 384 | bytes 3072 | tf_op jit(solution)/shard_map/psum | solution.py:125
  192.7 0.2 subtract_multiply_fusion
  192.9 1.3 collective-permute-start
  194.2 5.5 %convert_bitcast_fusion.1 = bf16[1,896,2048]{2,1,0:T(8,128)(2,1)} fusion(bf16[480,896]{1,0:T(8,128)(2,1)S(1)} %copy-done.18, bf16[480,2048]{1,0:T(8,128)(2,1)} %all-gather.6.cloned.1.call-done), kind=kOutput, calls=%fused_computation.44 | convolution fusion | flops 1763442688 | bytes 6496256 | tf_op jit(solution)/shard_map/dot_general | solution.py:35
  199.8 2.5 fusion.20
  202.3 41.1 %reduce-scatter.5.cloned.1.call-done = bf16[256,512]{1,0:T(8,128)(2,1)} async-done(((bf16[2048,512]{1,0:T(8,128)(2,1)}), bf16[256,512]{1,0:T(8,128)(2,1)}) %reduce-scatter.5.cloned.1.call-update) | async-done | bytes 262160 | tf_op jit(solution)/shard_map/reduce_scatter | solution.py:116
  243.4 1.8 convert_element_type.72
  (73 shorter events, 2.0 us)
Async XLA Ops:
  8.0 7.2 %copy-start = (bf16[192,512]{1,0:T(8,128)(2,1)S(1)}, bf16[192,512]{1,0:T(8,128)(2,1)}, u32[]{:S(2)}) copy-start(bf16[192,512]{1,0:T(8,128)(2,1)} %param.14) | copy-start | bytes 589828
  8.0 4.5 %copy-start.6 = (f32[192,2]{0,1:T(2,128)S(1)}, f32[192,2]{0,1:T(2,128)}, u32[]{:S(2)}) copy-start(f32[192,2]{0,1:T(2,128)} %param.17) | copy-start | bytes 4612
  8.0 53.3 %all-gather.6.cloned.1.call-start = ((), (), s32[]{:S(2)}) async-start(), calls=%async_computation.6 | async-start | bytes 2457600 | tf_op jit(solution)/shard_map/all_gather | solution.py:86
  40.3 45.0 %all-gather.4.cloned.1.call-start = ((), (), s32[]{:S(2)}) async-start(), calls=%async_computation.5 | async-start | bytes 2457600 | tf_op jit(solution)/shard_map/all_gather | solution.py:87
  58.8 72.6 %reduce-scatter.3.cloned.1.call-start = ((), (), s32[]{:S(2)}) async-start(), calls=%async_computation.7 | async-start | bytes 2457600 | tf_op jit(solution)/shard_map/reduce_scatter | solution.py:92
  66.2 29.7 %copy-start.15 = (f32[480,896]{1,0:T(8,128)}, f32[480,896]{1,0:T(8,128)S(1)}, u32[]{:S(2)}) copy-start(f32[480,896]{1,0:T(8,128)S(1)} %fusion.6) | copy-start | bytes 5160964
  85.3 6.0 %copy-start.9 = (bf16[1,896,2048]{2,1,0:T(8,128)(2,1)S(1)}, bf16[1,896,2048]{2,1,0:T(8,128)(2,1)}, u32[]{:S(2)}) copy-start(bf16[1,896,2048]{2,1,0:T(8,128)(2,1)} %param.19) | copy-start | bytes 11010052
  90.5 0.9 copy-start.17
  91.4 2.2 copy-start.11
  93.6 3.5 %copy-start.10 = (bf16[1,896,2048]{2,1,0:T(8,128)(2,1)S(1)}, bf16[1,896,2048]{2,1,0:T(8,128)(2,1)}, u32[]{:S(2)}) copy-start(bf16[1,896,2048]{2,1,0:T(8,128)(2,1)} %param.18) | copy-start | bytes 11010052
  95.9 1.2 copy-start.16
  100.8 38.2 %copy-start.5 = (s32[192,2]{0,1:T(2,128)S(1)}, s32[192,2]{0,1:T(2,128)}, u32[]{:S(2)}) copy-start(s32[192,2]{0,1:T(2,128)} %param.16) | copy-start | bytes 4612
  100.9 82.4 %all-gather.8.cloned.1.call-start = ((), (), s32[]{:S(2)}) async-start(), calls=%async_computation.9 | async-start | bytes 2359296 | tf_op jit(solution)/shard_map/all_gather | solution.py:112
  133.3 28.1 %all-to-all-start.2 = ((bf16[8,60,512]{2,1,0:T(8,128)(2,1)}), bf16[8,60,512]{2,1,0:T(8,128)(2,1)S(1)}, u32[]{:S(2)}, u32[]{:S(2)}) async-start(bf16[8,60,512]{2,1,0:T(8,128)(2,1)} %all_to_all.24), calls=%async_computation.3 | async-start | bytes 1048576 | tf_op jit(solution)/shard_map/all_to_all | solution.py:98
  138.8 104.6 %reduce-scatter.5.cloned.1.call-start = ((), (), s32[]{:S(2)}) async-start(), calls=%async_computation.8 | async-start | bytes 2359296 | tf_op jit(solution)/shard_map/reduce_scatter | solution.py:116
  161.5 3.4 %copy-start.1 = (bf16[192,512]{1,0:T(8,128)(2,1)S(1)}, bf16[192,512]{1,0:T(8,128)(2,1)}, u32[]{:S(2)}) copy-start(bf16[192,512]{1,0:T(8,128)(2,1)} %param.15) | copy-start | bytes 589828
  163.6 9.8 %copy-start.3 = (bf16[192,512]{1,0:T(8,128)(2,1)S(1)}, bf16[192,512]{1,0:T(8,128)(2,1)}, u32[]{:S(2)}) copy-start(bf16[192,512]{1,0:T(8,128)(2,1)} %param.21) | copy-start | bytes 589828
  163.6 9.8 %copy-start.7 = (f32[192]{0:T(256)S(1)}, f32[192]{0:T(256)}, u32[]{:S(2)}) copy-start(f32[192]{0:T(256)} %param.23) | copy-start | bytes 2308
  163.6 9.8 %copy-start.8 = (f32[192]{0:T(256)S(1)}, f32[192]{0:T(256)}, u32[]{:S(2)}) copy-start(f32[192]{0:T(256)} %param.22) | copy-start | bytes 2308
  163.6 9.8 %copy-start.13 = (f32[512]{0:T(512)S(1)}, f32[512]{0:T(512)}, u32[]{:S(2)}) copy-start(f32[512]{0:T(512)} %param.25) | copy-start | bytes 6148
  163.6 9.8 %copy-start.14 = (f32[512]{0:T(512)S(1)}, f32[512]{0:T(512)}, u32[]{:S(2)}) copy-start(f32[512]{0:T(512)} %param.24) | copy-start | bytes 6148
  165.0 10.7 %copy-start.2 = (bf16[192,512]{1,0:T(8,128)(2,1)}, bf16[192,512]{1,0:T(8,128)(2,1)S(1)}, u32[]{:S(2)}) copy-start(bf16[192,512]{1,0:T(8,128)(2,1)S(1)} %add_convert_fusion.1) | copy-start | bytes 589828
  175.7 0.8 copy-start.4
  175.7 1.6 copy-start.12
  183.3 10.9 %copy-start.18 = (bf16[480,896]{1,0:T(8,128)(2,1)S(1)}, bf16[480,896]{1,0:T(8,128)(2,1)}, u32[]{:S(2)}) copy-start(bf16[480,896]{1,0:T(8,128)(2,1)} %copy-done.17) | copy-start | bytes 2580484
  192.9 6.9 %collective-permute-start = (f32[30,512]{1,0:T(8,128)S(1)}, f32[30,512]{1,0:T(8,128)S(1)}, u32[]{:S(2)}, u32[]{:S(2)}) collective-permute-start(f32[30,512]{1,0:T(8,128)S(1)} %slice.263), channel_id=1, source_target_pairs={{4,0},{8,4},{12,8},{16,12},{20,16},{24,20},{28,24},{5,1},{9,5},{13... | collective-permute-start | bytes 184328 | tf_op jit(solution)/shard_map/ppermute | solution.py:10
Sparse Core Ops, SparseCore 0:
  40.4 20.8 all-gather.5
  63.5 21.8 all-gather.3
  101.0 30.3 reduce-scatter.2
Sparse Core Ops, SparseCore 1:
  103.5 58.3 all-gather.7
  175.8 67.5 reduce-scatter.4
where the time goes:
time: 253 us; the launch traced here: 252 us
  waiting for transfers between devices  115 us (45%)
  blocking collectives  54.5 us (22%)
  matrix products  34.5 us (14%)
  local copies, waits for them, and re-layouts  18.2 us (7%)
  between operations  15.6 us (6%)
  other arithmetic  7.48 us (3%)
  starting transfers between devices  7.19 us (3%)
    reduce_scatter x1, waiting for transfers between devices, on_device(): lax.psum_scatter(lax.dot_general(columns, activated, (((0,), (0,)), ((),...  41.1 us
    reduce_scatter x1, waiting for transfers between devices, on_device(): lax.psum_scatter(partial_rows.astype(jnp.bfloat16).astype(jnp.float32).as...  30 us
    all_to_all x1, waiting for transfers between devices, on_device(): lax.all_to_all(shared, 'sp', split_axis=0, concat_axis=0, tiled=True)  21.8 us
    all_to_all x1, blocking collectives, on_device(): lax.all_to_all(send_rows, 'sp', split_axis=0, concat_axis=0, tiled=True)  21.6 us
    all_gather x1, waiting for transfers between devices, on_device(): lax.all_gather(part_routed, 'tp', axis=1, tiled=True)  19.1 us
    all_to_all x1, blocking collectives, on_device(): lax.all_to_all(send_routed, 'sp', split_axis=0, concat_axis=0, tiled=True)  17.5 us
    all_gather x1, blocking collectives, on_device(): mix_grad = lax.all_gather(grad_stream, 'tp', axis=1, tiled=True)  8.42 us
    psum x1, blocking collectives, on_device(): lax.psum((jnp.sum(normed_grad, axis=1), jnp.sum(normed_grad * normed, axi...  6.95 us
  transfers between devices with their start and end apart: 7, of which 5 were waited for; matrix products, arithmetic and copies ran while one was open for 11% of the time, Pallas kernels for 0%

commit v1 on v0

--- a/solution.py
+++ b/solution.py
@@ -84,7 +84,7 @@
     )
     expert_rows, routed_rows = (
         lax.all_gather(part_rows, "tp", axis=1, tiled=True),
-        lax.all_gather(part_routed, "tp", axis=1, tiled=True),
+        jnp.concatenate(lax.all_gather(part_routed, "tp"), axis=1),
     )
     grad_up, grad_down, partial_rows = expert_backward(
         expert_rows, routed_rows, w_gate[0], w_up[0], w_down[0]

time: 253 us -> 255 us (level)
  waiting for transfers between devices: 115 us -> 119 us
  matrix products: 34.5 us -> 31.7 us
    all_gather x1, waiting for transfers between devices: 2.32 us -> 22.2 us  [on_device(): lax.all_gather(part_rows, 'tp', axis=1, tiled=True)]
    all_gather x1, waiting for transfers between devices: 19.1 us -> 2.32 us  [on_device(): lax.all_gather(part_routed, 'tp')]
    all_to_all x1, blocking collectives: 21.6 us -> 17.5 us  [on_device(): lax.all_to_all(send_rows, 'sp', split_axis=0, concat_axis=0, tiled=True)]
    all_to_all x1, blocking collectives: 17.5 us -> 21.6 us  [on_device(): lax.all_to_all(send_routed, 'sp', split_axis=0, concat_axis=0, tiled=True)]
    dot_general x1, matrix products: 5.1 us -> 2.28 us  [expert_backward(): lax.dot_general(routed_rows, down_weight, (((1,), (1,)), ((), ())), prefe...]
  transfers between devices with their start and end apart: 7 -> 7, of which waited for: 5 -> 5; matrix products, arithmetic and copies ran while one was open for 11% -> 10% of each run, Pallas kernels for 0% -> 0%
where the time goes in v1:
time: 255 us
  waiting for transfers between devices  119 us (47%)
  blocking collectives  54.5 us (21%)
  matrix products  31.7 us (12%)
  local copies, waits for them, and re-layouts  19.4 us (8%)
  between operations  15.7 us (6%)
  other arithmetic  7.47 us (3%)
  starting transfers between devices  7.19 us (3%)
    reduce_scatter x1, waiting for transfers between devices, on_device(): lax.psum_scatter(lax.dot_general(columns, activated, (((0,), (0,)), ((),...  41.7 us
    reduce_scatter x1, waiting for transfers between devices, on_device(): lax.psum_scatter(partial_rows.astype(jnp.bfloat16).astype(jnp.float32).as...  30 us
    all_gather x1, waiting for transfers between devices, on_device(): lax.all_gather(part_rows, 'tp', axis=1, tiled=True)  22.2 us
    all_to_all x1, waiting for transfers between devices, on_device(): lax.all_to_all(shared, 'sp', split_axis=0, concat_axis=0, tiled=True)  21.8 us
    all_to_all x1, blocking collectives, on_device(): lax.all_to_all(send_routed, 'sp', split_axis=0, concat_axis=0, tiled=True)  21.6 us
    all_to_all x1, blocking collectives, on_device(): lax.all_to_all(send_rows, 'sp', split_axis=0, concat_axis=0, tiled=True)  17.5 us
    all_gather x1, blocking collectives, on_device(): mix_grad = lax.all_gather(grad_stream, 'tp', axis=1, tiled=True)  8.42 us
    psum x1, blocking collectives, on_device(): lax.psum((jnp.sum(normed_grad, axis=1), jnp.sum(normed_grad * normed, axi...  6.96 us
  transfers between devices with their start and end apart: 7, of which 5 were waited for; matrix products, arithmetic and copies ran while one was open for 10% of the time, Pallas kernels for 0%

profile of v1, /device:TPU:0, one launch (start us, length us, event | category | flops | bytes accessed | tf_op | source)
XLA Modules:
  0.0 254.5 jit_solution(7365819691560449141)
XLA Ops:
  8.1 0.8 copy.35
  9.2 0.9 reduce-window.6
  10.0 0.2 slice_reduce_fusion
  10.4 0.2 select_reduce_fusion
  10.6 0.2 fusion.15
  10.8 1.1 mul.435
  12.0 0.5 mul.436
  12.7 0.1 mul.433
  12.9 2.1 gather_fusion
  15.2 2.1 gather_fusion.1
  17.5 0.3 select_select_fusion
  17.8 21.6 %all_to_all.27 = bf16[8,60,512]{2,1,0:T(8,128)(2,1)S(1)} all-to-all(bf16[8,60,512]{2,1,0:T(8,128)(2,1)S(1)} %get-tuple-element.45), channel_id=1, replica_groups=mesh['sp'=8,'tp'=4] {'sp'}, dimensions={0} | all-to-all | bytes 983040 | tf_op jit(solution)/shard_map/all_to_all | solution.py:83
  39.4 0.9 all_gather.15
  40.4 17.5 %all_to_all.28 = bf16[8,60,512]{2,1,0:T(8,128)(2,1)S(1)} all-to-all(bf16[8,60,512]{2,1,0:T(8,128)(2,1)S(1)} %get-tuple-element.44), channel_id=1, replica_groups=mesh['sp'=8,'tp'=4] {'sp'}, dimensions={0} | all-to-all | bytes 983040 | tf_op jit(solution)/shard_map/all_to_all | solution.py:82
  57.9 0.9 all_to_all.20
  58.8 0.2 reduce-scatter.3.cloned.1.call-start
  59.0 2.3 all-gather.4.cloned.1.call-done
  61.4 1.8 copy.42
  63.2 22.2 %all-gather.6.cloned.1.call-done = bf16[480,2048]{1,0:T(8,128)(2,1)} async-done(((bf16[480,512]{1,0:T(8,128)(2,1)}), bf16[480,2048]{1,0:T(8,128)(2,1)}) %all-gather.6.cloned.1.call-update) | async-done | bytes 1966096 | tf_op jit(solution)/shard_map/all_gather | solution.py:86
  85.4 5.0 %fusion.6 = f32[480,896]{1,0:T(8,128)S(1)} fusion(bf16[480,2048]{1,0:T(8,128)(2,1)} %all-gather.6.cloned.1.call-done, bf16[1,896,2048]{2,1,0:T(8,128)(2,1)} %param.18), kind=kOutput, calls=%fused_computation.39 | convolution fusion | flops 1761607680 | bytes 7356416 | tf_op jit(solution)/shard_map/dot_general | solution.py:18
  90.4 2.3 multiply_convert_fusion.2
  92.7 1.0 copy-done.18
  93.7 2.2 fusion
  95.9 2.3 fusion.2
  98.2 1.2 copy-done.17
  99.4 3.7 %add_convert_fusion = bf16[480,2048]{1,0:T(8,128)(2,1)} fusion(f32[480,2048]{1,0:T(8,128)S(1)} %fusion, bf16[1,896,2048]{2,1,0:T(8,128)(2,1)S(1)} %copy-done.12, f32[480,896]{1,0:T(8,128)S(1)} %fusion.6, f32[480,896]{1,0:T(8,128)S(1)} %get-tuple-element.47, f32[480,896]{1,0:T(8,128)S(1)} %fusion.2), kind=kOutput, calls=%fused_computation.32 | convolution fusion | flops 1767874560 | bytes 14729216 | tf_op jit(solution)/shard_map/dot_general | solution.py:38
  103.2 0.5 all-gather.8.cloned.1.call-update
  103.7 30.0 %reduce-scatter.3.cloned.1.call-done = bf16[480,512]{1,0:T(8,128)(2,1)} async-done(((bf16[480,2048]{1,0:T(8,128)(2,1)}), bf16[480,512]{1,0:T(8,128)(2,1)}) %reduce-scatter.3.cloned.1.call-update) | async-done | bytes 491536 | tf_op jit(solution)/shard_map/reduce_scatter | solution.py:92
  133.7 1.9 all_to_all.21
  135.6 5.5 %all-to-all-start.2 = ((bf16[8,60,512]{2,1,0:T(8,128)(2,1)}), bf16[8,60,512]{2,1,0:T(8,128)(2,1)S(1)}, u32[]{:S(2)}, u32[]{:S(2)}) async-start(bf16[8,60,512]{2,1,0:T(8,128)(2,1)} %all_to_all.21), calls=%async_computation.3 | async-start | bytes 1048576 | tf_op jit(solution)/shard_map/all_to_all | solution.py:98
  141.5 0.1 mul.447
  141.7 0.2 copy.40
  141.9 21.8 %all-to-all-done.2 = bf16[8,60,512]{2,1,0:T(8,128)(2,1)S(1)} async-done(((bf16[8,60,512]{2,1,0:T(8,128)(2,1)}), bf16[8,60,512]{2,1,0:T(8,128)(2,1)S(1)}, u32[]{:S(2)}, u32[]{:S(2)}) %all-to-all-start.2) | async-done | bytes 491552 | tf_op jit(solution)/shard_map/all_to_all | solution.py:98
  163.8 2.1 gather_fusion.2
  165.9 0.2 gather.23
  166.1 1.1 convert_reduce_fusion
  167.3 8.4 %all_gather.18 = bf16[192,2048]{1,0:T(8,128)(2,1)S(1)} all-gather(bf16[192,512]{1,0:T(8,128)(2,1)S(1)} %add_convert_fusion.1), channel_id=1, replica_groups=mesh['sp'=8,'tp'=4] {'tp'}, dimensions={1}, use_global_device_ids=true | all-gather | bytes 983040 | tf_op jit(solution)/shard_map/all_gather | solution.py:104
  175.7 2.3 convolution_convert_fusion
  178.0 0.8 copy-done.5
  178.9 6.0 %convert_bitcast_fusion = bf16[1,896,2048]{2,1,0:T(8,128)(2,1)} fusion(bf16[480,2048]{1,0:T(8,128)(2,1)S(1)} %bitcast.78, f32[480,896]{1,0:T(8,128)} %copy-done.17, f32[480,896]{1,0:T(8,128)} %copy-done.16), kind=kOutput, calls=%fused_computation.43 | convolution fusion | flops 1766023168 | bytes 9076736 | tf_op jit(solution)/shard_map/dot_general | solution.py:30
  184.9 2.5 fusion.121
  187.4 7.0 %all-reduce = (f32[192]{0:T(256)S(1)}, f32[192]{0:T(256)S(1)}) all-reduce(f32[192]{0:T(256)S(1)} %get-tuple-element.6, f32[192]{0:T(256)S(1)} %get-tuple-element.5), channel_id=1, replica_groups=mesh['sp'=8,'tp'=4] {'tp'}, use_global_device_ids=true, to_apply=%region_11.12 | all-reduce | flops 384 | bytes 3072 | tf_op jit(solution)/shard_map/psum | solution.py:125
  194.3 0.2 subtract_multiply_fusion
  194.5 1.3 collective-permute-start
  195.8 5.5 %convert_bitcast_fusion.1 = bf16[1,896,2048]{2,1,0:T(8,128)(2,1)} fusion(bf16[480,896]{1,0:T(8,128)(2,1)S(1)} %copy-done.19, bf16[480,2048]{1,0:T(8,128)(2,1)} %all-gather.6.cloned.1.call-done), kind=kOutput, calls=%fused_computation.44 | convolution fusion | flops 1763442688 | bytes 6496256 | tf_op jit(solution)/shard_map/dot_general | solution.py:35
  201.3 2.5 fusion.20
  203.8 41.7 %reduce-scatter.5.cloned.1.call-done = bf16[256,512]{1,0:T(8,128)(2,1)} async-done(((bf16[2048,512]{1,0:T(8,128)(2,1)}), bf16[256,512]{1,0:T(8,128)(2,1)}) %reduce-scatter.5.cloned.1.call-update) | async-done | bytes 262160 | tf_op jit(solution)/shard_map/reduce_scatter | solution.py:116
  245.6 1.8 convert_element_type.72
  (76 shorter events, 2.0 us)
Async XLA Ops:
  8.0 7.2 %copy-start = (bf16[192,512]{1,0:T(8,128)(2,1)S(1)}, bf16[192,512]{1,0:T(8,128)(2,1)}, u32[]{:S(2)}) copy-start(bf16[192,512]{1,0:T(8,128)(2,1)} %param.14) | copy-start | bytes 589828
  8.0 4.5 %copy-start.7 = (f32[192,2]{0,1:T(2,128)S(1)}, f32[192,2]{0,1:T(2,128)}, u32[]{:S(2)}) copy-start(f32[192,2]{0,1:T(2,128)} %param.17) | copy-start | bytes 4612
  8.0 53.3 %all-gather.4.cloned.1.call-start = ((), (), s32[]{:S(2)}) async-start(), calls=%async_computation.5 | async-start | bytes 2457600 | tf_op jit(solution)/shard_map/all_gather | solution.py:87
  40.3 45.0 %all-gather.6.cloned.1.call-start = ((), (), s32[]{:S(2)}) async-start(), calls=%async_computation.6 | async-start | bytes 2457600 | tf_op jit(solution)/shard_map/all_gather | solution.py:86
  58.8 74.9 %reduce-scatter.3.cloned.1.call-start = ((), (), s32[]{:S(2)}) async-start(), calls=%async_computation.7 | async-start | bytes 2457600 | tf_op jit(solution)/shard_map/reduce_scatter | solution.py:92
  85.3 5.0 %copy-start.10 = (bf16[1,896,2048]{2,1,0:T(8,128)(2,1)S(1)}, bf16[1,896,2048]{2,1,0:T(8,128)(2,1)}, u32[]{:S(2)}) copy-start(bf16[1,896,2048]{2,1,0:T(8,128)(2,1)} %param.20) | copy-start | bytes 11010052
  90.4 7.9 %copy-start.16 = (f32[480,896]{1,0:T(8,128)}, f32[480,896]{1,0:T(8,128)S(1)}, u32[]{:S(2)}) copy-start(f32[480,896]{1,0:T(8,128)S(1)} %fusion.6) | copy-start | bytes 5160964
  90.4 3.3 %copy-start.11 = (bf16[1,896,2048]{2,1,0:T(8,128)(2,1)S(1)}, bf16[1,896,2048]{2,1,0:T(8,128)(2,1)}, u32[]{:S(2)}) copy-start(bf16[1,896,2048]{2,1,0:T(8,128)(2,1)} %param.19) | copy-start | bytes 11010052
  92.7 1.0 copy-start.18
  93.7 2.2 copy-start.13
  95.9 3.5 %copy-start.12 = (bf16[1,896,2048]{2,1,0:T(8,128)(2,1)S(1)}, bf16[1,896,2048]{2,1,0:T(8,128)(2,1)}, u32[]{:S(2)}) copy-start(bf16[1,896,2048]{2,1,0:T(8,128)(2,1)} %param.18) | copy-start | bytes 11010052
  98.2 1.2 copy-start.17
  103.1 38.2 %copy-start.6 = (s32[192,2]{0,1:T(2,128)S(1)}, s32[192,2]{0,1:T(2,128)}, u32[]{:S(2)}) copy-start(s32[192,2]{0,1:T(2,128)} %param.16) | copy-start | bytes 4612
  103.2 81.8 %all-gather.8.cloned.1.call-start = ((), (), s32[]{:S(2)}) async-start(), calls=%async_computation.9 | async-start | bytes 2359296 | tf_op jit(solution)/shard_map/all_gather | solution.py:112
  135.6 28.1 %all-to-all-start.2 = ((bf16[8,60,512]{2,1,0:T(8,128)(2,1)}), bf16[8,60,512]{2,1,0:T(8,128)(2,1)S(1)}, u32[]{:S(2)}, u32[]{:S(2)}) async-start(bf16[8,60,512]{2,1,0:T(8,128)(2,1)} %all_to_all.21), calls=%async_computation.3 | async-start | bytes 1048576 | tf_op jit(solution)/shard_map/all_to_all | solution.py:98
  141.1 104.5 %reduce-scatter.5.cloned.1.call-start = ((), (), s32[]{:S(2)}) async-start(), calls=%async_computation.8 | async-start | bytes 2359296 | tf_op jit(solution)/shard_map/reduce_scatter | solution.py:116
  163.8 3.4 %copy-start.1 = (bf16[192,512]{1,0:T(8,128)(2,1)S(1)}, bf16[192,512]{1,0:T(8,128)(2,1)}, u32[]{:S(2)}) copy-start(bf16[192,512]{1,0:T(8,128)(2,1)} %param.15) | copy-start | bytes 589828
  165.9 9.8 %copy-start.8 = (f32[192]{0:T(256)S(1)}, f32[192]{0:T(256)}, u32[]{:S(2)}) copy-start(f32[192]{0:T(256)} %param.23) | copy-start | bytes 2308
  165.9 9.8 %copy-start.9 = (f32[192]{0:T(256)S(1)}, f32[192]{0:T(256)}, u32[]{:S(2)}) copy-start(f32[192]{0:T(256)} %param.22) | copy-start | bytes 2308
  165.9 9.8 %copy-start.14 = (f32[512]{0:T(512)S(1)}, f32[512]{0:T(512)}, u32[]{:S(2)}) copy-start(f32[512]{0:T(512)} %param.25) | copy-start | bytes 6148
  165.9 9.8 %copy-start.15 = (f32[512]{0:T(512)S(1)}, f32[512]{0:T(512)}, u32[]{:S(2)}) copy-start(f32[512]{0:T(512)} %param.24) | copy-start | bytes 6148
  166.1 9.7 %copy-start.3 = (bf16[192,512]{1,0:T(8,128)(2,1)S(1)}, bf16[192,512]{1,0:T(8,128)(2,1)}, u32[]{:S(2)}) copy-start(bf16[192,512]{1,0:T(8,128)(2,1)} %param.21) | copy-start | bytes 589828
  167.3 10.7 %copy-start.2 = (bf16[192,512]{1,0:T(8,128)(2,1)}, bf16[192,512]{1,0:T(8,128)(2,1)S(1)}, u32[]{:S(2)}) copy-start(bf16[192,512]{1,0:T(8,128)(2,1)S(1)} %add_convert_fusion.1) | copy-start | bytes 589828
  178.0 0.8 copy-start.5
  178.9 6.0 %copy-start.4 = (bf16[192,512]{1,0:T(8,128)(2,1)S(1)}, bf16[192,512]{1,0:T(8,128)(2,1)}, u32[]{:S(2)}) copy-start(bf16[192,512]{1,0:T(8,128)(2,1)} %param.21) | copy-start | bytes 589828
  184.9 10.9 %copy-start.19 = (bf16[480,896]{1,0:T(8,128)(2,1)S(1)}, bf16[480,896]{1,0:T(8,128)(2,1)}, u32[]{:S(2)}) copy-start(bf16[480,896]{1,0:T(8,128)(2,1)} %copy-done.18) | copy-start | bytes 2580484
  194.5 6.8 %collective-permute-start = (f32[30,512]{1,0:T(8,128)S(1)}, f32[30,512]{1,0:T(8,128)S(1)}, u32[]{:S(2)}, u32[]{:S(2)}) collective-permute-start(f32[30,512]{1,0:T(8,128)S(1)} %slice.263), channel_id=1, source_target_pairs={{4,0},{8,4},{12,8},{16,12},{20,16},{24,20},{28,24},{5,1},{9,5},{13... | collective-permute-start | bytes 184328 | tf_op jit(solution)/shard_map/ppermute | solution.py:10
Sparse Core Ops, SparseCore 0:
  40.4 20.8 all-gather.3
  63.5 21.8 all-gather.5
  103.3 30.3 reduce-scatter.2
Sparse Core Ops, SparseCore 1:
  105.8 58.3 all-gather.7
  178.1 67.4 reduce-scatter.4
